TPU v7x, 32 devices: a whole 2x2x4 slice. The times are simulated.
32 devices in a mesh: ep: 8 (over z, y), tp: 4 (over x, core).
Axes of the slice: x: 2, y: 2, z: 4, core: 2. Of those that a mesh axis runs over, the one named last changes fastest.
Arguments:
- outer_gate: bfloat16 [4096, 2048], P('ep', 'tp'), may hold values from -6 to 6
- inner_gate: bfloat16 [4096, 2048], P('ep', 'tp'), may hold values from -6 to 6
- conv_values: bfloat16 [4096, 2048], P('ep', 'tp'), may hold values from -6 to 6
- conv_taps: bfloat16 [3, 2048], P(None, 'tp'), may hold values from -3 to 3
- out_weight: bfloat16 [2048, 2048], P('tp'), may hold values from -0.125 to 0.125
- moe_input: bfloat16 [4096, 2048], P(('ep', 'tp')), may hold values from -6 to 6
- norm_gain: bfloat16 [2048], replicated, may hold values from 0.099609375 to 1.8984375
- gate_proj: bfloat16 [8, 2048, 1024], P('ep', None, 'tp'), may hold values from -0.125 to 0.125
- up_proj: bfloat16 [8, 2048, 1024], P('ep', None, 'tp'), may hold values from -0.125 to 0.125
- down_proj: bfloat16 [8, 1024, 2048], P('ep', 'tp'), may hold values from -0.1875 to 0.1875
- shared_gate: bfloat16 [2048, 1024], P(None, 'tp'), may hold values from -0.125 to 0.125
- shared_up: bfloat16 [2048, 1024], P(None, 'tp'), may hold values from -0.125 to 0.125
- shared_down: bfloat16 [1024, 2048], P('tp'), may hold values from -0.1875 to 0.1875
- routes: int32 [4096, 2], P('ep'), may hold values from 0 to 7, all different within a row; in each aligned block of 128 rows (0 to 127, 128 to 255, ...) at most 64 rows name the same one
- route_weight: float32 [4096, 2], P('ep'), may hold values from 0.3 to 1.5
Outputs:
- mixer_out: bfloat16 [4096, 2048], P(('ep', 'tp'))
- expert_mix: bfloat16 [4096, 2048], P(('ep', 'tp'))
Inputs may be any that keep to these rules, and one draw needn't show every extreme that they name: `routes`: each row names 2 different experts. In the 128 rows of one device no expert is named more than 64 times, and in every draw some expert is named exactly 64 times in one device's rows.
All inputs are finite; a program needn't handle non-finite values.
Results may differ from a plain program's by a relative error of at most 0.012.
Values may be sent and summed in bfloat16 or wider, within the bound.
A program may use at most 128 MiB of HBM per device.

v0:
```python
import functools

import jax
import jax.numpy as jnp
from jax import lax
from jax.experimental import pallas as pl
from jax.experimental.pallas import tpu as pltpu
from jax.sharding import PartitionSpec as P

epsilon = 1e-06
MESH = pl.DeviceIdType.MESH
f32 = jnp.float32
bf16 = jnp.bfloat16
CHUNKS = 4


def dot(a, b):
    return jnp.dot(a, b, preferred_element_type=f32)


def kernel(
    dims,
    outer, inner, values, taps, out_w, tokens, gain, gate_p, up_p, down_p,
    sh_gate, sh_up, sh_down, routes, weights,
    mix_o, exp_o,
    l_outer, l_inner, l_values, halo, prod, l_out_w, l_sg, l_su, l_sd,
    gf, uf, df, nf, og, ld, hid, rt, rv,
    acc, parts, pairs, sums, arrived,
    loc_sem, halo_send, halo_recv, x_send, p_send, t_recv,
    d_send, d_recv, b_send, b_recv, r_send, r_recv, rx_send, rx_recv,
):
    ep, tp, cap = dims
    half = tp // 2
    e, t = lax.axis_index("ep"), lax.axis_index("tp")
    a, b = t // 2, lax.rem(t, 2)
    pair = (e, 2 * a + 1 - b)
    group, ch = l_inner.shape
    rows, width = tokens.shape
    slots = ep * cap
    cols = width // CHUNKS
    n_taps = taps.shape[0]

    def far(d):
        return 2 * lax.rem(a + d, half) + b

    def near(d):
        return 2 * lax.rem(a + half - d, half) + b

    def remote(src, dst, s, r, dev):
        return pltpu.make_async_remote_copy(
            src_ref=src, dst_ref=dst, send_sem=s, recv_sem=r, device_id=dev, device_id_type=MESH
        )

    barrier = pltpu.get_barrier_semaphore()

    def greet(d, _):
        pl.semaphore_signal(barrier, inc=1, device_id=(lax.rem(e + d, ep), t), device_id_type=MESH)
        return 0

    lax.fori_loop(1, ep, greet, 0)
    pl.semaphore_signal(barrier, inc=1, device_id=pair, device_id_type=MESH)
    for d in range(1, half):
        pl.semaphore_signal(barrier, inc=1, device_id=(e, far(d)), device_id_type=MESH)

    local = [
        pltpu.make_async_copy(s, d, loc_sem.at[i])
        for i, (s, d) in enumerate(
            (
                (inner, l_inner), (values, l_values), (outer, l_outer), (out_w, l_out_w),
                (sh_gate, l_sg), (sh_up, l_su), (sh_down, l_sd),
                (gate_p.at[0], gf.at[t]), (up_p.at[0], uf.at[t]), (down_p.at[0], df.at[t]),
            )
        )
    ]
    for c in local:
        c.start()

    pl.semaphore_wait(barrier, ep - 1 + 1 + half - 1)

    kinds = CHUNKS + 3
    n_kind = kinds - 1

    def land(k, s):
        if k == 0:
            return gf.at[s]
        if k == 1:
            return uf.at[s]
        if k == n_kind:
            return nf.at[s]
        return df.at[s, :, pl.ds((k - 2) * cols, cols)]

    def origin(k):
        if k == 0:
            return gate_p.at[0]
        if k == 1:
            return up_p.at[0]
        if k == n_kind:
            return nf.at[t]
        return down_p.at[0, :, pl.ds((k - 2) * cols, cols)]

    def x_copy(k, d):
        return remote(origin(k), land(k, t), x_send.at[k, d], t_recv.at[k, d], (e, far(d)))

    def pair_copy(k):
        return remote(origin(k), land(k, t), p_send.at[k, 0], t_recv.at[k, 0], pair)

    def forward_copy(k, d):
        s = near(d)
        return remote(land(k, s), land(k, s), p_send.at[k, d], t_recv.at[k, half - 1 + d], pair)

    def start_x(k):
        for d in range(1, half):
            x_copy(k, d).start()

    def forward(k):
        for d in range(1, half):
            x_copy(k, d).wait_recv()
            forward_copy(k, d).start()

    def wait_forwarded(k):
        for d in range(1, half):
            forward_copy(k, d).wait_recv()

    for k in range(4):
        start_x(k)
    mine = pl.ds(pl.multiple_of(t * rows, rows), rows)
    own_routes, own_w = routes[:, mine], weights[:, mine]
    slot = lax.broadcasted_iota(jnp.int32, (slots, rows), 0)
    expert = slot // cap
    place = (slot - expert * cap).astype(f32)
    hit = jnp.zeros((slots, rows), f32)
    for k in range(own_routes.shape[0]):
        hit = jnp.where(own_routes[k : k + 1, :] == expert, 1.0, hit)
    upper = lax.broadcasted_iota(jnp.int32, (rows, rows), 0) < lax.broadcasted_iota(
        jnp.int32, (rows, rows), 1
    )
    earlier = dot(hit.astype(bf16), jnp.where(upper, 1.0, 0.0).astype(bf16))
    chosen = jnp.where(earlier == place, hit, 0.0)
    sender = chosen.astype(bf16)

    scales = gain[...].astype(f32).reshape(1, width)

    def norm_rows(i, _):
        at = pl.ds(pl.multiple_of(i * 16, 16), 16)
        v = tokens[at, :].astype(f32)
        square = jnp.mean(v * v, axis=-1, keepdims=True)
        nf[t, at, :] = (v * lax.rsqrt(square + epsilon) * scales).astype(bf16)
        return 0

    lax.fori_loop(0, rows // 16, norm_rows, 0)

    def block(i):
        return pl.ds(pl.multiple_of(i * cap, cap), cap)

    def dispatch_copy(c, d):
        to = lax.rem(e + d, ep)
        at = pl.ds(c * cols, cols)
        return remote(
            og.at[block(to), at], ld.at[block(e), at], d_send.at[c, d], d_recv.at[c, d], (to, t)
        )

    for c in range(CHUNKS):
        at = pl.ds(c * cols, cols)
        og[:, at] = dot(sender, nf[t, :, at]).astype(bf16)

        def start_dispatch(d, _):
            dispatch_copy(c, d).start()
            return 0

        lax.fori_loop(1, ep, start_dispatch, 0)
        ld[block(e), at] = og[block(e), at]
    start_x(n_kind)
    for k in range(kinds):
        pair_copy(k).start()
    for k in range(4, n_kind):
        start_x(k)
    edge = pl.ds(group - 16, 16)
    halos = [
        remote(src.at[edge, :], halo.at[i], halo_send.at[i], halo_recv.at[i], (lax.rem(e + 1, ep), t))
        for i, src in enumerate((inner, values))
    ]
    for c in halos:
        c.start()


    def pair_sum(j, i):
        return remote(
            parts.at[j, 2 * i + 1 - b], pairs.at[j, i], r_send.at[j, i], r_recv.at[j, i], pair
        )

    def far_sum(j, d):
        return remote(
            sums.at[j, d - 1], arrived.at[j, d - 1], rx_send.at[j, d], rx_recv.at[j, d], (e, far(d))
        )

    def start_far(j):
        for d in range(1, half):
            i = lax.rem(a + d, half)
            pair_sum(j, i).wait_recv()
            for c in range(CHUNKS):
                at = pl.ds(c * cols, cols)
                total = parts[j, 2 * i + b, :, at].astype(f32) + pairs[j, i, :, at].astype(f32)
                sums[j, d - 1, :, at] = total.astype(bf16)
            far_sum(j, d).start()

    def finish_sum(j):
        pair_sum(j, a).wait_recv()
        for d in range(1, half):
            far_sum(j, d).wait_recv()

    def summed(j, at):
        total = parts[j, t, :, at].astype(f32) + pairs[j, a, :, at].astype(f32)
        for d in range(1, half):
            total = total + arrived[j, d - 1, :, at].astype(f32)
        return total

    for c in local[:4]:
        c.wait()
    for c in halos:
        c.wait_recv()
    before = halo[0].astype(f32) * halo[1].astype(f32)
    prod[0:16, :] = jnp.where(e > 0, before, 0.0)
    prod[16:, :] = l_inner[...].astype(f32) * l_values[...].astype(f32)
    tap = taps[...].astype(f32)
    for s in range(tp):
        lo = s * rows
        conv = jnp.zeros((rows, ch), f32)
        for j in range(n_taps):
            first = 16 + lo - (n_taps - 1) + j
            conv = conv + tap[j : j + 1, :] * prod[first : first + rows, :]
        gated = (l_outer[lo : lo + rows, :].astype(f32) * conv).astype(bf16)
        for c in range(CHUNKS):
            at = pl.ds(c * cols, cols)
            parts[0, s, :, at] = dot(gated, l_out_w[:, at]).astype(bf16)
    for i in range(half):
        pair_sum(0, i).start()

    for c in local[4:]:
        c.wait()

    def shared(s):
        x = nf[s]
        g = dot(x, l_sg[...])
        u = dot(x, l_su[...])
        h = (g / (1.0 + jnp.exp(-g)) * u).astype(bf16)
        for c in range(CHUNKS):
            at = pl.ds(c * cols, cols)
            parts[1, s, :, at] = dot(h, l_sd[:, at]).astype(bf16)

    shared(t)
    pair_copy(n_kind).wait_recv()
    shared(2 * a + 1 - b)
    pair_sum(1, a).start()

    def act(s, g, u):
        hid[s] = (g / (1.0 + jnp.exp(-g)) * u).astype(bf16)

    pair_copy(0).wait_recv()
    pair_copy(1).wait_recv()
    close = (t, 2 * a + 1 - b)
    for c in range(CHUNKS):
        at = pl.ds(c * cols, cols)

        def wait_dispatch(d, _):
            dispatch_copy(c, d).wait_recv()
            return 0

        lax.fori_loop(1, ep, wait_dispatch, 0)
        for i, s in enumerate(close):
            g, u = dot(ld[:, at], gf[s, at, :]), dot(ld[:, at], uf[s, at, :])
            if c:
                g, u = g + acc[i, 0], u + acc[i, 1]
            if c < CHUNKS - 1:
                acc[i, 0] = g
                acc[i, 1] = u
            else:
                act(s, g, u)
        if c == 1:
            forward(0)
    wait_forwarded(0)
    rest = [near(d) for d in range(1, half)] + [near(d) + 1 - 2 * b for d in range(1, half)]
    gates = [dot(ld[...], gf[s]) for s in rest]
    forward(1)
    for n, s in enumerate(rest):
        if n == half - 1:
            wait_forwarded(1)
        act(s, gates[n], dot(ld[...], uf[s]))

    def back_copy(c, d):
        to = lax.rem(e + d, ep)
        at = pl.ds(c * cols, cols)
        return remote(
            rt.at[block(to), at], rv.at[block(e), at], b_send.at[c, d], b_recv.at[c, d], (to, t)
        )

    for c in range(CHUNKS):
        k = 2 + c
        at = pl.ds(c * cols, cols)
        pair_copy(k).wait_recv()
        forward(k)
        wait_forwarded(k)
        total = dot(hid[0], df[0, :, at])
        for s in range(1, tp):
            total = total + dot(hid[s], df[s, :, at])
        rt[:, at] = total.astype(bf16)

        def start_back(d, _):
            back_copy(c, d).start()
            return 0

        lax.fori_loop(1, ep, start_back, 0)
        rv[block(e), at] = rt[block(e), at]
        if c == 1:
            forward(n_kind)
            for d in range(1, half):
                shared(near(d))
            wait_forwarded(n_kind)
            for d in range(1, half):
                shared(near(d) + 1 - 2 * b)
                pair_sum(1, lax.rem(a + half - d, half)).start()
            start_far(1)
            start_far(0)

    scale = jnp.zeros((slots, rows), f32)
    for k in range(own_routes.shape[0]):
        scale = jnp.where(own_routes[k : k + 1, :] == expert, own_w[k : k + 1, :], scale)
    w_all = jnp.transpose(chosen * scale)
    w_hi = w_all.astype(bf16)
    w_lo = (w_all - w_hi.astype(f32)).astype(bf16)
    finish_sum(1)
    for c in range(CHUNKS):
        at = pl.ds(c * cols, cols)

        def wait_back(d, _):
            back_copy(c, d).wait_recv()
            return 0

        lax.fori_loop(1, ep, wait_back, 0)
        routed = dot(w_hi, rv[:, at]) + dot(w_lo, rv[:, at])
        exp_o[:, at] = (summed(1, at) + routed).astype(bf16)

    finish_sum(0)
    for c in range(CHUNKS):
        at = pl.ds(c * cols, cols)
        mix_o[:, at] = summed(0, at).astype(bf16)
    def sent(d, _):
        for c in range(CHUNKS):
            dispatch_copy(c, d).wait_send()
            back_copy(c, d).wait_send()
        return 0

    lax.fori_loop(1, ep, sent, 0)
    for c in halos:
        c.wait_send()
    for k in range(kinds):
        pair_copy(k).wait_send()
        for d in range(1, half):
            x_copy(k, d).wait_send()
            forward_copy(k, d).wait_send()
    for j in range(2):
        for i in range(half):
            pair_sum(j, i).wait_send()
        for d in range(1, half):
            far_sum(j, d).wait_send()


def per_device(
    outer_gate, inner_gate, conv_values, conv_taps, out_weight, moe_input, norm_gain,
    gate_proj, up_proj, down_proj, shared_gate, shared_up, shared_down, routes, route_weight,
):
    tp = lax.axis_size("tp")
    ep = lax.axis_size("ep")
    half = tp // 2
    group, ch = inner_gate.shape
    rows, width = moe_input.shape
    units = gate_proj.shape[2]
    sh_units = shared_gate.shape[1]
    cap = 2 * rows * routes.shape[1] // ep
    cap = -(-cap // 16) * 16
    slots = ep * cap
    kinds = CHUNKS + 3
    any_spec = pl.BlockSpec(memory_space=pl.ANY)
    vmem = pl.BlockSpec(memory_space=pltpu.VMEM)
    dma = pltpu.SemaphoreType.DMA

    def buf(*shape):
        return pltpu.VMEM(shape, bf16)

    scratch = [
        buf(group, ch), buf(group, ch), buf(group, ch), buf(2, 16, ch),
        pltpu.VMEM((group + 16, ch), f32), buf(ch, width),
        buf(width, sh_units), buf(width, sh_units), buf(sh_units, width),
        buf(tp, width, units), buf(tp, width, units), buf(tp, units, width),
        buf(tp, rows, width), buf(slots, width), buf(slots, width),
        buf(tp, slots, units), buf(slots, width), buf(slots, width),
        pltpu.VMEM((2, 2, slots, units), f32), buf(2, tp, rows, width), buf(2, half, rows, width),
        buf(2, half - 1, rows, width), buf(2, half - 1, rows, width),
        dma((10,)), dma((2,)), dma((2,)), dma((kinds, half)), dma((kinds, half)),
        dma((kinds, tp)), dma((CHUNKS, ep)), dma((CHUNKS, ep)), dma((CHUNKS, ep)), dma((CHUNKS, ep)),
        dma((2, half)), dma((2, half)), dma((2, half)), dma((2, half)),
    ]
    out = pltpu.VMEM((rows, width), bf16)
    return pl.pallas_call(
        functools.partial(kernel, (ep, tp, cap)),
        out_shape=(out, out),
        in_specs=[
            any_spec, any_spec, any_spec, vmem, any_spec, vmem, vmem,
            any_spec, any_spec, any_spec, any_spec, any_spec, any_spec, vmem, vmem,
        ],
        out_specs=(vmem, vmem),
        scratch_shapes=scratch,
        compiler_params=pltpu.CompilerParams(
            collective_id=0, has_side_effects=True, vmem_limit_bytes=65536000
        ),
    )(
        outer_gate, inner_gate, conv_values, conv_taps, out_weight, moe_input,
        norm_gain, gate_proj, up_proj, down_proj,
        shared_gate, shared_up, shared_down, routes.T, route_weight.T,
    )


def solution(mesh):
    return jax.shard_map(
        per_device,
        mesh=mesh,
        in_specs=(
            P("ep", "tp"), P("ep", "tp"), P("ep", "tp"), P(None, "tp"), P("tp", None),
            P(("ep", "tp"), None), P(),
            P("ep", None, "tp"), P("ep", None, "tp"), P("ep", "tp", None),
            P(None, "tp"), P(None, "tp"), P("tp", None), P("ep", None), P("ep", None),
        ),
        out_specs=(P(("ep", "tp"), None), P(("ep", "tp"), None)),
        check_vma=False,
    )
```

profile of v0, /device:TPU:0, one launch (start us, length us, event | category | flops | bytes accessed | tf_op | source)
XLA Modules:
  0.0 114.8 jit_solution(2362242550939017188)
XLA Ops:
  0.6 112.5 %shard_map.158 = (bf16[128,2048]{1,0:T(8,128)(2,1)S(1)}, bf16[128,2048]{1,0:T(8,128)(2,1)S(1)}) custom-call(bf16[512,512]{1,0:T(8,128)(2,1)} %outer.1, bf16[512,512]{1,0:T(8,128)(2,1)} %inner.1, bf16[512,512]{1,0:T(8,128)(2,1)} %values.1, bf16[3,512]{1,0:T(4,128)(2,1)} %taps.1, bf16[512,2048]{1,0:T(8,128)(2,1)} %out_w.1, bf16[128,2048]{1,0:T(8,128)(2,1)} %tokens.1, ...), custom_call_target="tpu_custom_call" | custom-call | tf_op jit(solution)/shard_map/pallas_call | solution.py:403
  113.2 0.8 copy.19
  114.0 0.8 copy.20
where the time goes:
time: 115 us
  Pallas kernels  113 us (98%)
  local copies, waits for them, and re-layouts  1.59 us (1%)
    pallas_call x1, Pallas kernels, per_device(): pl.pallas_call(functools.partial(kernel, (ep, tp, cap)), out_shape=(out,...  113 us

commit v1 on v0

--- a/solution.py
+++ b/solution.py
@@ -12,6 +12,8 @@
 f32 = jnp.float32
 bf16 = jnp.bfloat16
 CHUNKS = 4
+MERGED = 3
+NORMED_AT = 2
 
 
 def dot(a, b):
@@ -23,11 +25,15 @@
     outer, inner, values, taps, out_w, tokens, gain, gate_p, up_p, down_p,
     sh_gate, sh_up, sh_down, routes, weights,
     mix_o, exp_o,
+    l_tokens, l_gain, l_taps, l_routes, l_weights,
     l_outer, l_inner, l_values, halo, prod, l_out_w, l_sg, l_su, l_sd,
     gf, uf, df, nf, og, ld, hid, rt, rv,
     acc, parts, pairs, sums, arrived,
     loc_sem, halo_send, halo_recv, x_send, p_send, t_recv,
     d_send, d_recv, b_send, b_recv, r_send, r_recv, rx_send, rx_recv,
+    ready_up, ready_down,
+    g_routes, g_weights, g_blocks, g_rows, g_in, own_mix, gate_mix,
+    gr_send, gr_recv, hb_send, hb_recv, g_send, g_recv, m_send, m_recv,
 ):
     ep, tp, cap = dims
     half = tp // 2
@@ -53,15 +59,66 @@
 
     barrier = pltpu.get_barrier_semaphore()
 
-    def greet(d, _):
-        pl.semaphore_signal(barrier, inc=1, device_id=(lax.rem(e + d, ep), t), device_id_type=MESH)
-        return 0
-
-    lax.fori_loop(1, ep, greet, 0)
-    pl.semaphore_signal(barrier, inc=1, device_id=pair, device_id_type=MESH)
+    def signal(sem, dev):
+        pl.semaphore_signal(sem, inc=1, device_id=dev, device_id_type=MESH)
+
+    levels = ep // 2
+    level = e // 2
+    below, above = level > 0, level < levels - 1
+    lower, upper_dev = (jnp.maximum(e - 2, 0), t), (jnp.minimum(e + 2, ep - 1), t)
+    signal(barrier, pair)
     for d in range(1, half):
-        pl.semaphore_signal(barrier, inc=1, device_id=(e, far(d)), device_id_type=MESH)
-
+        signal(barrier, (e, far(d)))
+    chain = levels <= 4
+    if chain:
+        signal(barrier, (e + 1 - 2 * lax.rem(e, 2), t))
+
+        @pl.when(below)
+        def _():
+            signal(barrier, lower)
+
+        @pl.when(above)
+        def _():
+            signal(barrier, upper_dev)
+    else:
+
+        def greet(d, _):
+            signal(barrier, (lax.rem(e + d, ep), t))
+            return 0
+
+        lax.fori_loop(1, ep, greet, 0)
+
+    def ready_step(k):
+        if not chain:
+            return
+
+        @pl.when(above)
+        def _():
+            signal(ready_up.at[k], upper_dev)
+
+        @pl.when(below)
+        def _():
+            signal(ready_down.at[k], lower)
+
+        @pl.when(below)
+        def _():
+            pl.semaphore_wait(ready_up.at[k], 1)
+
+        @pl.when(above)
+        def _():
+            pl.semaphore_wait(ready_down.at[k], 1)
+
+    small = [
+        pltpu.make_async_copy(s, d, loc_sem.at[10 + i])
+        for i, (s, d) in enumerate(
+            (
+                (tokens, l_tokens), (gain, l_gain), (routes, l_routes), (weights, l_weights),
+                (taps, l_taps),
+            )
+        )
+    ]
+    for c in small:
+        c.start()
     local = [
         pltpu.make_async_copy(s, d, loc_sem.at[i])
         for i, (s, d) in enumerate(
@@ -75,7 +132,10 @@
     for c in local:
         c.start()
 
-    pl.semaphore_wait(barrier, ep - 1 + 1 + half - 1)
+    if chain:
+        pl.semaphore_wait(barrier, half + 1 + below.astype(jnp.int32) + above.astype(jnp.int32))
+    else:
+        pl.semaphore_wait(barrier, half + ep - 1)
 
     kinds = CHUNKS + 3
     n_kind = kinds - 1
@@ -121,33 +181,54 @@
         for d in range(1, half):
             forward_copy(k, d).wait_recv()
 
-    for k in range(4):
+    for k in range(3 + NORMED_AT):
         start_x(k)
+    ready_step(0)
+    for c in small:
+        c.wait()
     mine = pl.ds(pl.multiple_of(t * rows, rows), rows)
-    own_routes, own_w = routes[:, mine], weights[:, mine]
-    slot = lax.broadcasted_iota(jnp.int32, (slots, rows), 0)
-    expert = slot // cap
-    place = (slot - expert * cap).astype(f32)
-    hit = jnp.zeros((slots, rows), f32)
-    for k in range(own_routes.shape[0]):
-        hit = jnp.where(own_routes[k : k + 1, :] == expert, 1.0, hit)
-    upper = lax.broadcasted_iota(jnp.int32, (rows, rows), 0) < lax.broadcasted_iota(
-        jnp.int32, (rows, rows), 1
-    )
-    earlier = dot(hit.astype(bf16), jnp.where(upper, 1.0, 0.0).astype(bf16))
-    chosen = jnp.where(earlier == place, hit, 0.0)
+    own_routes, own_w = l_routes[:, mine], l_weights[:, mine]
+
+    def table(named, first, count):
+        slot = lax.broadcasted_iota(jnp.int32, (count * cap, rows), 0)
+        index = slot // cap
+        place = (slot - index * cap).astype(f32)
+        expert = index + first
+        hit = jnp.zeros((count * cap, rows), f32)
+        for k in range(named.shape[0]):
+            hit = jnp.where(named[k : k + 1, :] == expert, 1.0, hit)
+        upper = lax.broadcasted_iota(jnp.int32, (rows, rows), 0) < lax.broadcasted_iota(
+            jnp.int32, (rows, rows), 1
+        )
+        earlier = dot(hit.astype(bf16), jnp.where(upper, 1.0, 0.0).astype(bf16))
+        return jnp.where(earlier == place, hit, 0.0), expert
+
+    def weighted(chosen, expert, named, given):
+        scale = jnp.zeros(chosen.shape, f32)
+        for k in range(named.shape[0]):
+            scale = jnp.where(named[k : k + 1, :] == expert, given[k : k + 1, :], scale)
+        full = jnp.transpose(chosen * scale)
+        high = full.astype(bf16)
+        return high, (full - high.astype(f32)).astype(bf16)
+
+    chosen, expert = table(own_routes, 0, ep)
     sender = chosen.astype(bf16)
 
-    scales = gain[...].astype(f32).reshape(1, width)
+    if levels > 2:
+        ready_step(1)
+    scales = l_gain[...].astype(f32).reshape(1, width)
 
     def norm_rows(i, _):
         at = pl.ds(pl.multiple_of(i * 16, 16), 16)
-        v = tokens[at, :].astype(f32)
+        v = l_tokens[at, :].astype(f32)
         square = jnp.mean(v * v, axis=-1, keepdims=True)
         nf[t, at, :] = (v * lax.rsqrt(square + epsilon) * scales).astype(bf16)
         return 0
 
     lax.fori_loop(0, rows // 16, norm_rows, 0)
+
+    for k in range(2, levels - 1):
+        ready_step(k)
 
     def block(i):
         return pl.ds(pl.multiple_of(i * cap, cap), cap)
@@ -172,8 +253,24 @@
     start_x(n_kind)
     for k in range(kinds):
         pair_copy(k).start()
-    for k in range(4, n_kind):
+    for k in range(3 + NORMED_AT, n_kind):
         start_x(k)
+    here = e // 4
+    place4 = lax.rem(e, 4)
+    line = lax.rem(e, 2)
+    inner_level = lax.rem(level, 2)
+    is_gate = level == 1 + here
+    other_gate = (jnp.minimum(2 * (2 - here) + line, ep - 1), t)
+
+    def table_copies(i):
+        return [
+            remote(src.at[:, mine], dst.at[i], gr_send.at[n], gr_recv.at[n, i], other_gate)
+            for n, (src, dst) in enumerate(((l_routes, g_routes), (l_weights, g_weights)))
+        ]
+
+    if chain:
+        for c in table_copies(inner_level):
+            c.start()
     edge = pl.ds(group - 16, 16)
     halos = [
         remote(src.at[edge, :], halo.at[i], halo_send.at[i], halo_recv.at[i], (lax.rem(e + 1, ep), t))
@@ -188,9 +285,11 @@
             parts.at[j, 2 * i + 1 - b], pairs.at[j, i], r_send.at[j, i], r_recv.at[j, i], pair
         )
 
-    def far_sum(j, d):
-        return remote(
-            sums.at[j, d - 1], arrived.at[j, d - 1], rx_send.at[j, d], rx_recv.at[j, d], (e, far(d))
+    def far_sum(j, d, c):
+        at = pl.ds(c * cols, cols)
+        return remote(
+            sums.at[j, d - 1, :, at], arrived.at[j, d - 1, :, at],
+            rx_send.at[j, d, c], rx_recv.at[j, d, c], (e, far(d)),
         )
 
     def start_far(j):
@@ -201,14 +300,12 @@
                 at = pl.ds(c * cols, cols)
                 total = parts[j, 2 * i + b, :, at].astype(f32) + pairs[j, i, :, at].astype(f32)
                 sums[j, d - 1, :, at] = total.astype(bf16)
-            far_sum(j, d).start()
-
-    def finish_sum(j):
-        pair_sum(j, a).wait_recv()
+                far_sum(j, d, c).start()
+
+    def summed(j, c):
+        at = pl.ds(c * cols, cols)
         for d in range(1, half):
-            far_sum(j, d).wait_recv()
-
-    def summed(j, at):
+            far_sum(j, d, c).wait_recv()
         total = parts[j, t, :, at].astype(f32) + pairs[j, a, :, at].astype(f32)
         for d in range(1, half):
             total = total + arrived[j, d - 1, :, at].astype(f32)
@@ -221,7 +318,7 @@
     before = halo[0].astype(f32) * halo[1].astype(f32)
     prod[0:16, :] = jnp.where(e > 0, before, 0.0)
     prod[16:, :] = l_inner[...].astype(f32) * l_values[...].astype(f32)
-    tap = taps[...].astype(f32)
+    tap = l_taps[...].astype(f32)
     for s in range(tp):
         lo = s * rows
         conv = jnp.zeros((rows, ch), f32)
@@ -293,6 +390,107 @@
             rt.at[block(to), at], rv.at[block(e), at], b_send.at[c, d], b_recv.at[c, d], (to, t)
         )
 
+    def near_copy(c, i):
+        to = 4 * here + lax.rem(place4 + i, 4)
+        at = pl.ds(c * cols, cols)
+        return remote(
+            rt.at[block(to), at], rv.at[block(e), at], hb_send.at[c, i], hb_recv.at[c, i], (to, t)
+        )
+
+    def gate_of(j):
+        return 2 * (1 + here) + j % 2
+
+    def gate_copy(c, j):
+        at = pl.ds(c * cols, cols)
+        return remote(
+            rt.at[block(4 - 4 * here + j), at], g_blocks.at[j // 2, block(place4), at],
+            g_send.at[c, j], g_recv.at[c, j // 2, place4], (gate_of(j), t),
+        )
+
+    def gate_arrival(c, i, r):
+        at = pl.ds(c * cols, cols)
+        return remote(
+            rt.at[block(0), at], g_blocks.at[i, block(r), at],
+            g_send.at[c, i], g_recv.at[c, i, r], (gate_of(0), t),
+        )
+
+    def row_copy(c, i):
+        at = pl.ds(c * cols, cols)
+        return remote(
+            g_rows.at[i, :, at], g_in.at[:, at], m_send.at[c, i], m_recv.at[c],
+            (4 - 4 * here + 2 * i + line, t),
+        )
+
+    def start_back(c):
+        at = pl.ds(c * cols, cols)
+        if chain and c < MERGED:
+            for j in range(4):
+
+                @pl.when(gate_of(j) != e)
+                def _():
+                    gate_copy(c, j).start()
+
+                @pl.when(gate_of(j) == e)
+                def _():
+                    g_blocks[j // 2, block(place4), at] = rt[block(4 - 4 * here + j), at]
+
+            for i in range(1, 4):
+                near_copy(c, i).start()
+        else:
+
+            def start_one(d, _):
+                back_copy(c, d).start()
+                return 0
+
+            lax.fori_loop(1, ep, start_one, 0)
+        rv[block(e), at] = rt[block(e), at]
+
+    def wait_back(c):
+        if chain and c < MERGED:
+            for i in range(1, 4):
+                near_copy(c, i).wait_recv()
+            row_copy(c, 0).wait_recv()
+        else:
+
+            def wait_one(d, _):
+                back_copy(c, d).wait_recv()
+                return 0
+
+            lax.fori_loop(1, ep, wait_one, 0)
+
+    def merge(c):
+        if not chain or c >= MERGED:
+            return
+        at = pl.ds(c * cols, cols)
+
+        @pl.when(is_gate)
+        def _():
+            for i in range(2):
+                for r in range(1, 4):
+                    gate_arrival(c, i, lax.rem(place4 + r, 4)).wait_recv()
+                blocks = g_blocks[i, :, at]
+                rows_in = dot(gate_mix[i, 0], blocks) + dot(gate_mix[i, 1], blocks)
+                g_rows[i, :, at] = rows_in.astype(bf16)
+                row_copy(c, i).start()
+
+    if chain:
+        mix = weighted(chosen, expert, own_routes, own_w)
+        wide = 4 * cap
+        for h in range(2):
+            for n in range(2):
+                own_mix[h, n] = mix[n][:, h * wide : (h + 1) * wide]
+
+        @pl.when(is_gate)
+        def _():
+            for i in range(2):
+                for c in table_copies(i):
+                    c.wait_recv()
+                named = g_routes[i]
+                picked, which = table(named, 4 * here, 4)
+                pair_of = weighted(picked, which, named, g_weights[i])
+                for n in range(2):
+                    gate_mix[i, n] = pair_of[n]
+
     for c in range(CHUNKS):
         k = 2 + c
         at = pl.ds(c * cols, cols)
@@ -303,14 +501,11 @@
         for s in range(1, tp):
             total = total + dot(hid[s], df[s, :, at])
         rt[:, at] = total.astype(bf16)
-
-        def start_back(d, _):
-            back_copy(c, d).start()
-            return 0
-
-        lax.fori_loop(1, ep, start_back, 0)
-        rv[block(e), at] = rt[block(e), at]
-        if c == 1:
+        start_back(c)
+        if c > 0:
+            merge(c - 1)
+        if c == NORMED_AT:
+            start_far(0)
             forward(n_kind)
             for d in range(1, half):
                 shared(near(d))
@@ -319,34 +514,53 @@
                 shared(near(d) + 1 - 2 * b)
                 pair_sum(1, lax.rem(a + half - d, half)).start()
             start_far(1)
-            start_far(0)
-
-    scale = jnp.zeros((slots, rows), f32)
-    for k in range(own_routes.shape[0]):
-        scale = jnp.where(own_routes[k : k + 1, :] == expert, own_w[k : k + 1, :], scale)
-    w_all = jnp.transpose(chosen * scale)
-    w_hi = w_all.astype(bf16)
-    w_lo = (w_all - w_hi.astype(f32)).astype(bf16)
-    finish_sum(1)
+    merge(CHUNKS - 1)
+
+    if not chain:
+        mix = weighted(chosen, expert, own_routes, own_w)
+    pair_sum(1, a).wait_recv()
     for c in range(CHUNKS):
         at = pl.ds(c * cols, cols)
-
-        def wait_back(d, _):
-            back_copy(c, d).wait_recv()
-            return 0
-
-        lax.fori_loop(1, ep, wait_back, 0)
-        routed = dot(w_hi, rv[:, at]) + dot(w_lo, rv[:, at])
-        exp_o[:, at] = (summed(1, at) + routed).astype(bf16)
-
-    finish_sum(0)
+        wait_back(c)
+        if chain:
+            routed = jnp.zeros((rows, cols), f32)
+            for h in (here, 1 - here)[: 1 if c < MERGED else 2]:
+                got = rv[pl.ds(pl.multiple_of(h * wide, wide), wide), at]
+                routed = routed + (dot(own_mix[h, 0], got) + dot(own_mix[h, 1], got))
+            if c < MERGED:
+                routed = routed + g_in[:, at].astype(f32)
+        else:
+            routed = dot(mix[0], rv[:, at]) + dot(mix[1], rv[:, at])
+        exp_o[:, at] = (summed(1, c) + routed).astype(bf16)
+
+    pair_sum(0, a).wait_recv()
     for c in range(CHUNKS):
         at = pl.ds(c * cols, cols)
-        mix_o[:, at] = summed(0, at).astype(bf16)
+        mix_o[:, at] = summed(0, c).astype(bf16)
+
+    if chain:
+        for c in table_copies(inner_level):
+            c.wait_send()
+        for c in range(MERGED):
+            for j in range(4):
+
+                @pl.when(gate_of(j) != e)
+                def _():
+                    gate_copy(c, j).wait_send()
+
+            for i in range(1, 4):
+                near_copy(c, i).wait_send()
+
+            @pl.when(is_gate)
+            def _():
+                for i in range(2):
+                    row_copy(c, i).wait_send()
+
     def sent(d, _):
         for c in range(CHUNKS):
             dispatch_copy(c, d).wait_send()
-            back_copy(c, d).wait_send()
+            if not chain or c >= MERGED:
+                back_copy(c, d).wait_send()
         return 0
 
     lax.fori_loop(1, ep, sent, 0)
@@ -360,8 +574,9 @@
     for j in range(2):
         for i in range(half):
             pair_sum(j, i).wait_send()
-        for d in range(1, half):
-            far_sum(j, d).wait_send()
+        for c in range(CHUNKS):
+            for d in range(1, half):
+                far_sum(j, d, c).wait_send()
 
 
 def per_device(
@@ -379,14 +594,16 @@
     cap = -(-cap // 16) * 16
     slots = ep * cap
     kinds = CHUNKS + 3
+    vmem = pl.BlockSpec(memory_space=pltpu.VMEM)
     any_spec = pl.BlockSpec(memory_space=pl.ANY)
-    vmem = pl.BlockSpec(memory_space=pltpu.VMEM)
     dma = pltpu.SemaphoreType.DMA
 
     def buf(*shape):
         return pltpu.VMEM(shape, bf16)
 
     scratch = [
+        buf(rows, width), buf(width), buf(*conv_taps.shape),
+        pltpu.VMEM((routes.shape[1], group), jnp.int32), pltpu.VMEM((routes.shape[1], group), f32),
         buf(group, ch), buf(group, ch), buf(group, ch), buf(2, 16, ch),
         pltpu.VMEM((group + 16, ch), f32), buf(ch, width),
         buf(width, sh_units), buf(width, sh_units), buf(sh_units, width),
@@ -395,18 +612,23 @@
         buf(tp, slots, units), buf(slots, width), buf(slots, width),
         pltpu.VMEM((2, 2, slots, units), f32), buf(2, tp, rows, width), buf(2, half, rows, width),
         buf(2, half - 1, rows, width), buf(2, half - 1, rows, width),
-        dma((10,)), dma((2,)), dma((2,)), dma((kinds, half)), dma((kinds, half)),
+        dma((15,)), dma((2,)), dma((2,)), dma((kinds, half)), dma((kinds, half)),
         dma((kinds, tp)), dma((CHUNKS, ep)), dma((CHUNKS, ep)), dma((CHUNKS, ep)), dma((CHUNKS, ep)),
-        dma((2, half)), dma((2, half)), dma((2, half)), dma((2, half)),
+        dma((2, half)), dma((2, half)), dma((2, half, CHUNKS)), dma((2, half, CHUNKS)),
+        pltpu.SemaphoreType.REGULAR((max(ep // 2 - 1, 1),)),
+        pltpu.SemaphoreType.REGULAR((max(ep // 2 - 1, 1),)),
+        pltpu.VMEM((2, routes.shape[1], rows), jnp.int32),
+        pltpu.VMEM((2, routes.shape[1], rows), f32),
+        buf(2, 4 * cap, width), buf(2, rows, width), buf(rows, width),
+        buf(2, 2, rows, 4 * cap), buf(2, 2, rows, 4 * cap),
+        dma((2,)), dma((2, 2)), dma((CHUNKS, 4)), dma((CHUNKS, 4)),
+        dma((CHUNKS, 4)), dma((CHUNKS, 2, 4)), dma((CHUNKS, 2)), dma((CHUNKS,)),
     ]
     out = pltpu.VMEM((rows, width), bf16)
     return pl.pallas_call(
         functools.partial(kernel, (ep, tp, cap)),
         out_shape=(out, out),
-        in_specs=[
-            any_spec, any_spec, any_spec, vmem, any_spec, vmem, vmem,
-            any_spec, any_spec, any_spec, any_spec, any_spec, any_spec, vmem, vmem,
-        ],
+        in_specs=[any_spec] * 15,
         out_specs=(vmem, vmem),
         scratch_shapes=scratch,
         compiler_params=pltpu.CompilerParams(

time: 115 us -> 112 us (0.974)
  Pallas kernels: 113 us -> 110 us
    pallas_call x1, Pallas kernels: 113 us -> 110 us  [per_device(): pl.pallas_call(functools.partial(kernel, (ep, tp, cap)), out_shape=(out,...]
where the time goes in v1:
time: 112 us
  Pallas kernels  110 us (98%)
  local copies, waits for them, and re-layouts  1.59 us (1%)
    pallas_call x1, Pallas kernels, per_device(): pl.pallas_call(functools.partial(kernel, (ep, tp, cap)), out_shape=(out,...  110 us

profile of v1, /device:TPU:0, one launch (start us, length us, event | category | flops | bytes accessed | tf_op | source)
XLA Modules:
  0.0 112.1 jit_solution(10661199671221484509)
XLA Ops:
  0.6 109.9 %shard_map.158 = (bf16[128,2048]{1,0:T(8,128)(2,1)S(1)}, bf16[128,2048]{1,0:T(8,128)(2,1)S(1)}) custom-call(bf16[512,512]{1,0:T(8,128)(2,1)} %outer.1, bf16[512,512]{1,0:T(8,128)(2,1)} %inner.1, bf16[512,512]{1,0:T(8,128)(2,1)} %values.1, bf16[3,512]{1,0:T(4,128)(2,1)} %taps.1, bf16[512,2048]{1,0:T(8,128)(2,1)} %out_w.1, bf16[128,2048]{1,0:T(8,128)(2,1)} %tokens.1, ...), custom_call_target="tpu_custom_call" | custom-call | tf_op jit(solution)/shard_map/pallas_call | solution.py:628
  110.5 0.8 copy.19
  111.3 0.8 copy.20

commit v2 on v1

--- a/solution.py
+++ b/solution.py
@@ -12,8 +12,9 @@
 f32 = jnp.float32
 bf16 = jnp.bfloat16
 CHUNKS = 4
-MERGED = 3
 NORMED_AT = 2
+SPREAD_AT = 0
+FAR_AT = 3
 
 
 def dot(a, b):
@@ -29,11 +30,15 @@
     l_outer, l_inner, l_values, halo, prod, l_out_w, l_sg, l_su, l_sd,
     gf, uf, df, nf, og, ld, hid, rt, rv,
     acc, parts, pairs, sums, arrived,
-    loc_sem, halo_send, halo_recv, x_send, p_send, t_recv,
-    d_send, d_recv, b_send, b_recv, r_send, r_recv, rx_send, rx_recv,
+    loc_sem, sent_sem, halo_recv, t_recv,
+    d_send, d_recv, b_send, b_recv, r_recv, rx_recv,
     ready_up, ready_down,
     g_routes, g_weights, g_blocks, g_rows, g_in, own_mix, gate_mix,
-    gr_send, gr_recv, hb_send, hb_recv, g_send, g_recv, m_send, m_recv,
+    gr_recv, b_in, g_recv,
+    g_tokens, g_slots, gate_pick,
+    d_in, raw_recv,
+    far_g, far_u, far_d, sh_hid,
+    px_recv, pn_recv, pg_recv, py_recv, pf_recv, pa_recv, pb_recv,
 ):
     ep, tp, cap = dims
     half = tp // 2
@@ -158,15 +163,24 @@
             return nf.at[t]
         return down_p.at[0, :, pl.ds((k - 2) * cols, cols)]
 
+    to_gate, to_slots, to_back, to_rows, to_pieces, to_spread, to_forward = range(7)
+    to_x, to_pair, to_relay, to_sums, to_halo, to_table = 7, 8, 9, 10, 11, 13
+
+    def group_of(i):
+        return sent_sem.at[i]
+
+    def drain(i, ref):
+        remote(ref, ref, group_of(i), group_of(i), pair).wait_send()
+
     def x_copy(k, d):
-        return remote(origin(k), land(k, t), x_send.at[k, d], t_recv.at[k, d], (e, far(d)))
+        return remote(origin(k), land(k, t), group_of(to_x), t_recv.at[k, d], (e, far(d)))
 
     def pair_copy(k):
-        return remote(origin(k), land(k, t), p_send.at[k, 0], t_recv.at[k, 0], pair)
+        return remote(origin(k), land(k, t), group_of(to_gate if chain and k == n_kind else to_pair), t_recv.at[k, 0], pair)
 
     def forward_copy(k, d):
         s = near(d)
-        return remote(land(k, s), land(k, s), p_send.at[k, d], t_recv.at[k, half - 1 + d], pair)
+        return remote(land(k, s), land(k, s), group_of(to_relay), t_recv.at[k, half - 1 + d], pair)
 
     def start_x(k):
         for d in range(1, half):
@@ -181,7 +195,102 @@
         for d in range(1, half):
             forward_copy(k, d).wait_recv()
 
-    for k in range(3 + NORMED_AT):
+    here = e // 4
+    place4 = lax.rem(e, 4)
+    line = lax.rem(e, 2)
+    inner_level = lax.rem(level, 2)
+    is_gate = level == 1 + here
+    other_gate = (jnp.minimum(2 * (2 - here) + line, ep - 1), t)
+    beside = (e + 1 - 2 * line, t)
+    partner_e = e + 2 - 4 * inner_level
+    partner = (jnp.minimum(partner_e, ep - 1), t)
+
+    def away(i, y):
+        return 4 - 4 * here + 2 * i + y
+
+    unit = sh_down.shape[0] // ep
+
+    def piece(w, d, i):
+        ref = (far_g, far_u, far_d)[w].at[d - 1]
+        n = ref.shape[0] // ep
+        return ref.at[pl.ds(pl.multiple_of(i * n, n), n), :]
+
+    def piece_x(w, d):
+        src = (sh_gate, sh_up, sh_down)[w]
+        n = src.shape[0] // ep
+        return remote(
+            src.at[pl.ds(pl.multiple_of(e * n, n), n), :], piece(w, d, e),
+            group_of(to_pieces), px_recv.at[w, d - 1], (e, far(d)),
+        )
+
+    def piece_partner(w, d, i):
+        return remote(piece(w, d, i), piece(w, d, i), group_of(to_spread), pn_recv.at[w, d - 1], partner)
+
+    beside_e = e + 1 - 2 * line
+
+    def piece_gate(w, d, k):
+        p = piece(w, d, (e, beside_e)[k])
+        arrived_sem = pa_recv.at[d - 1] if k else pg_recv.at[w, d - 1]
+        return remote(p, p, group_of(to_spread), arrived_sem, other_gate)
+
+    def piece_forward(w, d, i):
+        p = piece(w, d, away(i, line))
+        return remote(p, p, group_of(to_forward), pf_recv.at[w, d - 1], partner)
+
+    def piece_beside(w, d, j):
+        p = piece(w, d, (e, partner_e, away(0, line), away(1, line))[j])
+        arrived_sem = py_recv.at[d - 1] if j else pb_recv.at[w, d - 1]
+        return remote(p, p, group_of(to_pieces), arrived_sem, beside)
+
+    pieces = [(w, d) for w in range(3) for d in range(1, half)] if chain else []
+
+    def spread_own():
+        for w, d in pieces:
+            piece_x(w, d).wait_recv()
+            piece_gate(w, d, 0).start()
+            piece_partner(w, d, e).start()
+            piece_beside(w, d, 0).start()
+
+    def spread_partner():
+        for w, d in pieces:
+            piece_beside(w, d, 0).wait_recv()
+            piece_gate(w, d, 1).start()
+        for w, d in pieces:
+            piece_partner(w, d, partner_e).wait_recv()
+            piece_beside(w, d, 1).start()
+
+    def spread_away(gates):
+        @pl.when(is_gate if gates else jnp.logical_not(is_gate))
+        def _():
+            for w, d in pieces:
+                n = (far_g, far_u, far_d)[w].shape[1] // ep
+                both = (far_g, far_u, far_d)[w].at[d - 1, pl.ds(0, 2 * n), :]
+                arrived_sem = (pg_recv if gates else pf_recv).at[w, d - 1]
+                remote(both, both, group_of(to_spread), arrived_sem, partner).wait_recv()
+                for i in range(2):
+                    if gates:
+                        piece_forward(w, d, i).start()
+                    else:
+                        piece_beside(w, d, 2 + i).start()
+
+    def wait_pieces():
+        for d in range(1, half):
+
+            @pl.when(is_gate)
+            def _():
+                for count, sem in ((3, py_recv), (6, pa_recv)):
+                    some = og.at[pl.ds(0, count * unit), :]
+                    remote(some, some, group_of(to_pieces), sem.at[d - 1], beside).wait_recv()
+
+            @pl.when(jnp.logical_not(is_gate))
+            def _():
+                some = og.at[pl.ds(0, 9 * unit), :]
+                remote(some, some, group_of(to_pieces), py_recv.at[d - 1], beside).wait_recv()
+
+    if chain:
+        for w, d in pieces:
+            piece_x(w, d).start()
+    for k in range(n_kind if chain else 3 + NORMED_AT):
         start_x(k)
     ready_step(0)
     for c in small:
@@ -230,66 +339,109 @@
     for k in range(2, levels - 1):
         ready_step(k)
 
-    def block(i):
-        return pl.ds(pl.multiple_of(i * cap, cap), cap)
-
-    def dispatch_copy(c, d):
-        to = lax.rem(e + d, ep)
-        at = pl.ds(c * cols, cols)
-        return remote(
-            og.at[block(to), at], ld.at[block(e), at], d_send.at[c, d], d_recv.at[c, d], (to, t)
-        )
-
-    for c in range(CHUNKS):
-        at = pl.ds(c * cols, cols)
-        og[:, at] = dot(sender, nf[t, :, at]).astype(bf16)
-
-        def start_dispatch(d, _):
-            dispatch_copy(c, d).start()
-            return 0
-
-        lax.fori_loop(1, ep, start_dispatch, 0)
-        ld[block(e), at] = og[block(e), at]
-    start_x(n_kind)
-    for k in range(kinds):
-        pair_copy(k).start()
-    for k in range(3 + NORMED_AT, n_kind):
-        start_x(k)
-    here = e // 4
-    place4 = lax.rem(e, 4)
-    line = lax.rem(e, 2)
-    inner_level = lax.rem(level, 2)
-    is_gate = level == 1 + here
-    other_gate = (jnp.minimum(2 * (2 - here) + line, ep - 1), t)
-
     def table_copies(i):
         return [
-            remote(src.at[:, mine], dst.at[i], gr_send.at[n], gr_recv.at[n, i], other_gate)
+            remote(src.at[:, mine], dst.at[i], group_of(to_table + n), gr_recv.at[n], other_gate)
             for n, (src, dst) in enumerate(((l_routes, g_routes), (l_weights, g_weights)))
         ]
 
-    if chain:
-        for c in table_copies(inner_level):
-            c.start()
     edge = pl.ds(group - 16, 16)
     halos = [
-        remote(src.at[edge, :], halo.at[i], halo_send.at[i], halo_recv.at[i], (lax.rem(e + 1, ep), t))
+        remote(src.at[edge, :], halo.at[i], group_of(to_halo + i), halo_recv.at[i], (lax.rem(e + 1, ep), t))
         for i, src in enumerate((inner, values))
     ]
     for c in halos:
         c.start()
+    if chain:
+        for c in table_copies(inner_level):
+            c.start()
+
+    def block(i):
+        return pl.ds(pl.multiple_of(i * cap, cap), cap)
+
+    def near_dispatch(c, i):
+        to = 4 * here + lax.rem(place4 + i, 4)
+        at = pl.ds(c * cols, cols)
+        return remote(
+            og.at[block(to), at], ld.at[block(e), at], group_of(to_gate), d_in.at[c], (to, t)
+        )
+
+    def raw_copy(c, i):
+        at = pl.ds(c * cols, cols)
+        return remote(
+            nf.at[t, :, at], g_tokens.at[i, :, at], group_of(to_gate), raw_recv.at[c], other_gate
+        )
+
+    def slot_copy(c, i, r):
+        at = pl.ds(c * cols, cols)
+        return remote(
+            g_slots.at[i, block(r), at], ld.at[block(away(i, line)), at],
+            group_of(to_slots), d_in.at[c], (4 * here + r, t),
+        )
+
+    def forward_slots(c):
+        if not chain:
+            return
+        at = pl.ds(c * cols, cols)
+
+        @pl.when(is_gate)
+        def _():
+            both = g_slots.at[0, pl.ds(0, 2 * rows), at]
+            remote(both, both, group_of(to_gate), raw_recv.at[c], other_gate).wait_recv()
+            for i in range(2):
+                g_slots[i, :, at] = dot(gate_pick[i], g_tokens[i, :, at]).astype(bf16)
+                for r in range(4):
+
+                    @pl.when(place4 != r)
+                    def _():
+                        slot_copy(c, i, r).start()
+
+                ld[block(away(i, line)), at] = g_slots[i, block(place4), at]
+
+    def dispatch_copy(c, d):
+        to = lax.rem(e + d, ep)
+        at = pl.ds(c * cols, cols)
+        return remote(
+            og.at[block(to), at], ld.at[block(e), at], d_send.at[c, d], d_recv.at[c, d], (to, t)
+        )
+
+    for c in range(CHUNKS):
+        at = pl.ds(c * cols, cols)
+        og[:, at] = dot(sender, nf[t, :, at]).astype(bf16)
+
+        if chain:
+            raw_copy(c, inner_level).start()
+            for i in range(1, 4):
+                near_dispatch(c, i).start()
+        else:
+
+            def start_dispatch(d, _):
+                dispatch_copy(c, d).start()
+                return 0
+
+            lax.fori_loop(1, ep, start_dispatch, 0)
+        ld[block(e), at] = og[block(e), at]
+    if not chain:
+        start_x(n_kind)
+    for k in range(kinds):
+        pair_copy(k).start()
+    if chain:
+        spread_own()
+    else:
+        for k in range(3 + NORMED_AT, n_kind):
+            start_x(k)
 
 
     def pair_sum(j, i):
         return remote(
-            parts.at[j, 2 * i + 1 - b], pairs.at[j, i], r_send.at[j, i], r_recv.at[j, i], pair
+            parts.at[j, 2 * i + 1 - b], pairs.at[j, i], group_of(to_sums), r_recv.at[j, i], pair
         )
 
     def far_sum(j, d, c):
         at = pl.ds(c * cols, cols)
         return remote(
             sums.at[j, d - 1, :, at], arrived.at[j, d - 1, :, at],
-            rx_send.at[j, d, c], rx_recv.at[j, d, c], (e, far(d)),
+            group_of(to_sums), rx_recv.at[j, d - 1, c], (e, far(d)),
         )
 
     def start_far(j):
@@ -304,12 +456,33 @@
 
     def summed(j, c):
         at = pl.ds(c * cols, cols)
+        total = parts[j, t, :, at].astype(f32) + pairs[j, a, :, at].astype(f32)
+        if chain and j == 1:
+            return total
         for d in range(1, half):
             far_sum(j, d, c).wait_recv()
-        total = parts[j, t, :, at].astype(f32) + pairs[j, a, :, at].astype(f32)
         for d in range(1, half):
             total = total + arrived[j, d - 1, :, at].astype(f32)
         return total
+
+    if chain:
+        mix = weighted(chosen, expert, own_routes, own_w)
+        wide = 4 * cap
+        for h in range(2):
+            for n in range(2):
+                own_mix[h, n] = mix[n][:, h * wide : (h + 1) * wide]
+
+        @pl.when(is_gate)
+        def _():
+            for n, ref in enumerate((g_routes, g_weights)):
+                remote(ref, ref, group_of(to_table + n), gr_recv.at[n], other_gate).wait_recv()
+            for i in range(2):
+                named = g_routes[i]
+                picked, which = table(named, 4 * here, 4)
+                pair_of = weighted(picked, which, named, g_weights[i])
+                gate_pick[i] = picked.astype(bf16)
+                for n in range(2):
+                    gate_mix[i, n] = pair_of[n]
 
     for c in local[:4]:
         c.wait()
@@ -329,8 +502,11 @@
         for c in range(CHUNKS):
             at = pl.ds(c * cols, cols)
             parts[0, s, :, at] = dot(gated, l_out_w[:, at]).astype(bf16)
+        if s == tp // 2 - 1:
+            forward_slots(0)
     for i in range(half):
         pair_sum(0, i).start()
+    forward_slots(1)
 
     for c in local[4:]:
         c.wait()
@@ -344,10 +520,40 @@
             at = pl.ds(c * cols, cols)
             parts[1, s, :, at] = dot(h, l_sd[:, at]).astype(bf16)
 
-    shared(t)
-    pair_copy(n_kind).wait_recv()
-    shared(2 * a + 1 - b)
-    pair_sum(1, a).start()
+    def shared_hidden(x, gate_w, up_w):
+        g = dot(x, gate_w)
+        u = dot(x, up_w)
+        return (g / (1.0 + jnp.exp(-g)) * u).astype(bf16)
+
+    couple = (t, 2 * a + 1 - b)
+    if chain:
+        sh_hid[0, 0] = shared_hidden(nf[t], l_sg[...], l_su[...])
+        forward_slots(2)
+        pair_copy(n_kind).wait_recv()
+        sh_hid[0, 1] = shared_hidden(nf[couple[1]], l_sg[...], l_su[...])
+        forward_slots(3)
+        spread_partner()
+        spread_away(True)
+    else:
+        shared(t)
+        pair_copy(n_kind).wait_recv()
+        shared(couple[1])
+        pair_sum(1, a).start()
+
+    def far_shared():
+        wait_pieces()
+        for i, s in enumerate(couple):
+            for d in range(1, half):
+                sh_hid[d, i] = shared_hidden(nf[s], far_g[d - 1], far_u[d - 1])
+        for i in (1, 0):
+            for c in range(CHUNKS):
+                at = pl.ds(c * cols, cols)
+                total = dot(sh_hid[0, i], l_sd[:, at])
+                for d in range(1, half):
+                    total = total + dot(sh_hid[d, i], far_d[d - 1, :, at])
+                parts[1, couple[i], :, at] = total.astype(bf16)
+            if i:
+                pair_sum(1, a).start()
 
     def act(s, g, u):
         hid[s] = (g / (1.0 + jnp.exp(-g)) * u).astype(bf16)
@@ -358,11 +564,21 @@
     for c in range(CHUNKS):
         at = pl.ds(c * cols, cols)
 
-        def wait_dispatch(d, _):
-            dispatch_copy(c, d).wait_recv()
-            return 0
-
-        lax.fori_loop(1, ep, wait_dispatch, 0)
+        if chain:
+            for count, mine_too in ((5, is_gate), (7, jnp.logical_not(is_gate))):
+
+                @pl.when(mine_too)
+                def _():
+                    blocks = ld.at[pl.ds(0, count * cap), at]
+                    remote(blocks, blocks, group_of(to_gate), d_in.at[c], pair).wait_recv()
+
+        else:
+
+            def wait_dispatch(d, _):
+                dispatch_copy(c, d).wait_recv()
+                return 0
+
+            lax.fori_loop(1, ep, wait_dispatch, 0)
         for i, s in enumerate(close):
             g, u = dot(ld[:, at], gf[s, at, :]), dot(ld[:, at], uf[s, at, :])
             if c:
@@ -391,10 +607,10 @@
         )
 
     def near_copy(c, i):
-        to = 4 * here + lax.rem(place4 + i, 4)
-        at = pl.ds(c * cols, cols)
-        return remote(
-            rt.at[block(to), at], rv.at[block(e), at], hb_send.at[c, i], hb_recv.at[c, i], (to, t)
+        to = e + (0, 1 - 2 * line, 2 - 4 * inner_level, 3 - 2 * line - 4 * inner_level)[i]
+        at = pl.ds(c * cols, cols)
+        return remote(
+            rt.at[block(to), at], rv.at[block(e), at], group_of(to_back), b_in.at[c], (to, t)
         )
 
     def gate_of(j):
@@ -404,26 +620,19 @@
         at = pl.ds(c * cols, cols)
         return remote(
             rt.at[block(4 - 4 * here + j), at], g_blocks.at[j // 2, block(place4), at],
-            g_send.at[c, j], g_recv.at[c, j // 2, place4], (gate_of(j), t),
-        )
-
-    def gate_arrival(c, i, r):
-        at = pl.ds(c * cols, cols)
-        return remote(
-            rt.at[block(0), at], g_blocks.at[i, block(r), at],
-            g_send.at[c, i], g_recv.at[c, i, r], (gate_of(0), t),
+            group_of(to_back), g_recv.at[c], (gate_of(j), t),
         )
 
     def row_copy(c, i):
         at = pl.ds(c * cols, cols)
         return remote(
-            g_rows.at[i, :, at], g_in.at[:, at], m_send.at[c, i], m_recv.at[c],
+            g_rows.at[i, :, at], g_in.at[:, at], group_of(to_rows), b_in.at[c],
             (4 - 4 * here + 2 * i + line, t),
         )
 
     def start_back(c):
         at = pl.ds(c * cols, cols)
-        if chain and c < MERGED:
+        if chain:
             for j in range(4):
 
                 @pl.when(gate_of(j) != e)
@@ -434,8 +643,17 @@
                 def _():
                     g_blocks[j // 2, block(place4), at] = rt[block(4 - 4 * here + j), at]
 
-            for i in range(1, 4):
-                near_copy(c, i).start()
+            for gate, now in ((True, (2, 3)), (False, (1,))):
+
+                @pl.when(is_gate if gate else jnp.logical_not(is_gate))
+                def _():
+                    for i in now:
+                        near_copy(c, i).start()
+                    for m in range(CHUNKS if c == CHUNKS - 1 else 0):
+                        for i in range(1, 4):
+                            if i not in now:
+                                near_copy(m, i).start()
+
         else:
 
             def start_one(d, _):
@@ -446,10 +664,9 @@
         rv[block(e), at] = rt[block(e), at]
 
     def wait_back(c):
-        if chain and c < MERGED:
-            for i in range(1, 4):
-                near_copy(c, i).wait_recv()
-            row_copy(c, 0).wait_recv()
+        if chain:
+            got = rt.at[pl.ds(0, 3 * cap + rows), pl.ds(c * cols, cols)]
+            remote(got, got, group_of(to_back), b_in.at[c], pair).wait_recv()
         else:
 
             def wait_one(d, _):
@@ -459,37 +676,19 @@
             lax.fori_loop(1, ep, wait_one, 0)
 
     def merge(c):
-        if not chain or c >= MERGED:
+        if not chain:
             return
         at = pl.ds(c * cols, cols)
 
         @pl.when(is_gate)
         def _():
+            six = rt.at[pl.ds(0, 6 * cap), at]
+            remote(six, six, group_of(to_back), g_recv.at[c], pair).wait_recv()
             for i in range(2):
-                for r in range(1, 4):
-                    gate_arrival(c, i, lax.rem(place4 + r, 4)).wait_recv()
                 blocks = g_blocks[i, :, at]
                 rows_in = dot(gate_mix[i, 0], blocks) + dot(gate_mix[i, 1], blocks)
                 g_rows[i, :, at] = rows_in.astype(bf16)
                 row_copy(c, i).start()
-
-    if chain:
-        mix = weighted(chosen, expert, own_routes, own_w)
-        wide = 4 * cap
-        for h in range(2):
-            for n in range(2):
-                own_mix[h, n] = mix[n][:, h * wide : (h + 1) * wide]
-
-        @pl.when(is_gate)
-        def _():
-            for i in range(2):
-                for c in table_copies(i):
-                    c.wait_recv()
-                named = g_routes[i]
-                picked, which = table(named, 4 * here, 4)
-                pair_of = weighted(picked, which, named, g_weights[i])
-                for n in range(2):
-                    gate_mix[i, n] = pair_of[n]
 
     for c in range(CHUNKS):
         k = 2 + c
@@ -504,7 +703,13 @@
         start_back(c)
         if c > 0:
             merge(c - 1)
-        if c == NORMED_AT:
+        if chain and c == 1:
+            start_far(0)
+        if chain and c == FAR_AT:
+            far_shared()
+        if chain and c == SPREAD_AT:
+            spread_away(False)
+        if not chain and c == NORMED_AT:
             start_far(0)
             forward(n_kind)
             for d in range(1, half):
@@ -520,52 +725,56 @@
         mix = weighted(chosen, expert, own_routes, own_w)
     pair_sum(1, a).wait_recv()
     for c in range(CHUNKS):
+        if c == CHUNKS - 1:
+            pair_sum(0, a).wait_recv()
+            for m in range(CHUNKS):
+                at = pl.ds(m * cols, cols)
+                mix_o[:, at] = summed(0, m).astype(bf16)
         at = pl.ds(c * cols, cols)
         wait_back(c)
         if chain:
-            routed = jnp.zeros((rows, cols), f32)
-            for h in (here, 1 - here)[: 1 if c < MERGED else 2]:
-                got = rv[pl.ds(pl.multiple_of(h * wide, wide), wide), at]
-                routed = routed + (dot(own_mix[h, 0], got) + dot(own_mix[h, 1], got))
-            if c < MERGED:
-                routed = routed + g_in[:, at].astype(f32)
+            got = rv[pl.ds(pl.multiple_of(here * wide, wide), wide), at]
+            routed = dot(own_mix[here, 0], got) + dot(own_mix[here, 1], got)
+            routed = routed + g_in[:, at].astype(f32)
         else:
             routed = dot(mix[0], rv[:, at]) + dot(mix[1], rv[:, at])
         exp_o[:, at] = (summed(1, c) + routed).astype(bf16)
 
-    pair_sum(0, a).wait_recv()
-    for c in range(CHUNKS):
-        at = pl.ds(c * cols, cols)
-        mix_o[:, at] = summed(0, c).astype(bf16)
-
+
+    for c in halos:
+        c.wait_send()
     if chain:
         for c in table_copies(inner_level):
             c.wait_send()
-        for c in range(MERGED):
-            for j in range(4):
-
-                @pl.when(gate_of(j) != e)
-                def _():
-                    gate_copy(c, j).wait_send()
-
-            for i in range(1, 4):
-                near_copy(c, i).wait_send()
-
-            @pl.when(is_gate)
-            def _():
-                for i in range(2):
-                    row_copy(c, i).wait_send()
+        drain(to_gate, og.at[pl.ds(0, 2 * rows + 3 * cap), :])
+        drain(to_spread, og.at[pl.ds(0, 9 * unit), :])
+        drain(to_x, gf.at[pl.ds(0, 3)])
+        drain(to_pair, gf.at[pl.ds(0, 3)])
+        drain(to_relay, gf.at[pl.ds(0, 3)])
+        drain(to_sums, og.at[pl.ds(0, 4 * rows), :])
+
+        @pl.when(is_gate)
+        def _():
+            drain(to_slots, og.at[pl.ds(0, 6 * cap), :])
+            drain(to_rows, og.at[pl.ds(0, 2 * rows), :])
+            drain(to_forward, og.at[pl.ds(0, 6 * unit), :])
+            drain(to_back, og.at[pl.ds(0, 5 * cap), :])
+            drain(to_pieces, og.at[pl.ds(0, 9 * unit), :])
+
+        @pl.when(jnp.logical_not(is_gate))
+        def _():
+            drain(to_back, og.at[pl.ds(0, 7 * cap), :])
+            drain(to_pieces, og.at[pl.ds(0, 15 * unit), :])
+
+        return
 
     def sent(d, _):
         for c in range(CHUNKS):
             dispatch_copy(c, d).wait_send()
-            if not chain or c >= MERGED:
-                back_copy(c, d).wait_send()
+            back_copy(c, d).wait_send()
         return 0
 
     lax.fori_loop(1, ep, sent, 0)
-    for c in halos:
-        c.wait_send()
     for k in range(kinds):
         pair_copy(k).wait_send()
         for d in range(1, half):
@@ -598,6 +807,8 @@
     any_spec = pl.BlockSpec(memory_space=pl.ANY)
     dma = pltpu.SemaphoreType.DMA
 
+    direct = (1, 1) if ep <= 8 else (CHUNKS, ep)
+
     def buf(*shape):
         return pltpu.VMEM(shape, bf16)
 
@@ -612,17 +823,22 @@
         buf(tp, slots, units), buf(slots, width), buf(slots, width),
         pltpu.VMEM((2, 2, slots, units), f32), buf(2, tp, rows, width), buf(2, half, rows, width),
         buf(2, half - 1, rows, width), buf(2, half - 1, rows, width),
-        dma((15,)), dma((2,)), dma((2,)), dma((kinds, half)), dma((kinds, half)),
-        dma((kinds, tp)), dma((CHUNKS, ep)), dma((CHUNKS, ep)), dma((CHUNKS, ep)), dma((CHUNKS, ep)),
-        dma((2, half)), dma((2, half)), dma((2, half, CHUNKS)), dma((2, half, CHUNKS)),
+        dma((15,)), dma((15,)), dma((2,)),
+        dma((kinds, 2 * half - 1)), dma(direct), dma(direct), dma(direct), dma(direct),
+        dma((2, half)), dma((2, half - 1, CHUNKS)),
         pltpu.SemaphoreType.REGULAR((max(ep // 2 - 1, 1),)),
         pltpu.SemaphoreType.REGULAR((max(ep // 2 - 1, 1),)),
         pltpu.VMEM((2, routes.shape[1], rows), jnp.int32),
         pltpu.VMEM((2, routes.shape[1], rows), f32),
         buf(2, 4 * cap, width), buf(2, rows, width), buf(rows, width),
         buf(2, 2, rows, 4 * cap), buf(2, 2, rows, 4 * cap),
-        dma((2,)), dma((2, 2)), dma((CHUNKS, 4)), dma((CHUNKS, 4)),
-        dma((CHUNKS, 4)), dma((CHUNKS, 2, 4)), dma((CHUNKS, 2)), dma((CHUNKS,)),
+        dma((2,)), dma((CHUNKS,)), dma((CHUNKS,)),
+        buf(2, rows, width), buf(2, 4 * cap, width), buf(2, 4 * cap, rows),
+        dma((CHUNKS,)), dma((CHUNKS,)),
+        buf(half - 1, width, sh_units), buf(half - 1, width, sh_units), buf(half - 1, sh_units, width),
+        buf(half, 2, rows, sh_units),
+        dma((3, half - 1)), dma((3, half - 1)), dma((3, half - 1)), dma((half - 1,)), dma((3, half - 1)),
+        dma((half - 1,)), dma((3, half - 1)),
     ]
     out = pltpu.VMEM((rows, width), bf16)
     return pl.pallas_call(

time: 112 us -> 105 us (0.938)
  the two profiles are of different devices: /device:TPU:0 before, /device:TPU:17 now
where the time goes in v2:
time: 105 us
  Pallas kernels  103 us (98%)
  local copies, waits for them, and re-layouts  1.59 us (2%)
    pallas_call x1, Pallas kernels, per_device(): pl.pallas_call(functools.partial(kernel, (ep, tp, cap)), out_shape=(out,...  103 us

profile of v2, /device:TPU:17, one launch (start us, length us, event | category | flops | bytes accessed | tf_op | source)
XLA Modules:
  0.0 105.2 jit_solution(11127791994967849457)
XLA Ops:
  0.6 102.9 %shard_map.158 = (bf16[128,2048]{1,0:T(8,128)(2,1)S(1)}, bf16[128,2048]{1,0:T(8,128)(2,1)S(1)}) custom-call(bf16[512,512]{1,0:T(8,128)(2,1)} %outer.1, bf16[512,512]{1,0:T(8,128)(2,1)} %inner.1, bf16[512,512]{1,0:T(8,128)(2,1)} %values.1, bf16[3,512]{1,0:T(4,128)(2,1)} %taps.1, bf16[512,2048]{1,0:T(8,128)(2,1)} %out_w.1, bf16[128,2048]{1,0:T(8,128)(2,1)} %tokens.1, ...), custom_call_target="tpu_custom_call" | custom-call | tf_op jit(solution)/shard_map/pallas_call | solution.py:844
  103.6 0.8 copy.19
  104.4 0.8 copy.20

commit v3 on v2

--- a/solution.py
+++ b/solution.py
@@ -12,9 +12,10 @@
 f32 = jnp.float32
 bf16 = jnp.bfloat16
 CHUNKS = 4
+RETURNS = 8
+LAG = 3
 NORMED_AT = 2
-SPREAD_AT = 0
-FAR_AT = 3
+SPREAD_AT = 2
 
 
 def dot(a, b):
@@ -49,6 +50,9 @@
     rows, width = tokens.shape
     slots = ep * cap
     cols = width // CHUNKS
+    returns = RETURNS if ep <= 8 else CHUNKS
+    lag = LAG if ep <= 8 else 1
+    bcols = width // returns
     n_taps = taps.shape[0]
 
     def far(d):
@@ -142,7 +146,7 @@
     else:
         pl.semaphore_wait(barrier, half + ep - 1)
 
-    kinds = CHUNKS + 3
+    kinds = returns + 3
     n_kind = kinds - 1
 
     def land(k, s):
@@ -152,7 +156,7 @@
             return uf.at[s]
         if k == n_kind:
             return nf.at[s]
-        return df.at[s, :, pl.ds((k - 2) * cols, cols)]
+        return df.at[s, :, pl.ds((k - 2) * bcols, bcols)]
 
     def origin(k):
         if k == 0:
@@ -161,7 +165,7 @@
             return up_p.at[0]
         if k == n_kind:
             return nf.at[t]
-        return down_p.at[0, :, pl.ds((k - 2) * cols, cols)]
+        return down_p.at[0, :, pl.ds((k - 2) * bcols, bcols)]
 
     to_gate, to_slots, to_back, to_rows, to_pieces, to_spread, to_forward = range(7)
     to_x, to_pair, to_relay, to_sums, to_halo, to_table = 7, 8, 9, 10, 11, 13
@@ -454,11 +458,12 @@
                 sums[j, d - 1, :, at] = total.astype(bf16)
                 far_sum(j, d, c).start()
 
+    def own_shared(at):
+        return parts[1, t, :, at].astype(f32) + pairs[1, a, :, at].astype(f32)
+
     def summed(j, c):
         at = pl.ds(c * cols, cols)
         total = parts[j, t, :, at].astype(f32) + pairs[j, a, :, at].astype(f32)
-        if chain and j == 1:
-            return total
         for d in range(1, half):
             far_sum(j, d, c).wait_recv()
         for d in range(1, half):
@@ -542,10 +547,9 @@
 
     def far_shared():
         wait_pieces()
-        for i, s in enumerate(couple):
+        for i in (1, 0):
             for d in range(1, half):
-                sh_hid[d, i] = shared_hidden(nf[s], far_g[d - 1], far_u[d - 1])
-        for i in (1, 0):
+                sh_hid[d, i] = shared_hidden(nf[couple[i]], far_g[d - 1], far_u[d - 1])
             for c in range(CHUNKS):
                 at = pl.ds(c * cols, cols)
                 total = dot(sh_hid[0, i], l_sd[:, at])
@@ -601,14 +605,14 @@
 
     def back_copy(c, d):
         to = lax.rem(e + d, ep)
-        at = pl.ds(c * cols, cols)
+        at = pl.ds(c * bcols, bcols)
         return remote(
             rt.at[block(to), at], rv.at[block(e), at], b_send.at[c, d], b_recv.at[c, d], (to, t)
         )
 
     def near_copy(c, i):
         to = e + (0, 1 - 2 * line, 2 - 4 * inner_level, 3 - 2 * line - 4 * inner_level)[i]
-        at = pl.ds(c * cols, cols)
+        at = pl.ds(c * bcols, bcols)
         return remote(
             rt.at[block(to), at], rv.at[block(e), at], group_of(to_back), b_in.at[c], (to, t)
         )
@@ -617,21 +621,21 @@
         return 2 * (1 + here) + j % 2
 
     def gate_copy(c, j):
-        at = pl.ds(c * cols, cols)
+        at = pl.ds(c * bcols, bcols)
         return remote(
             rt.at[block(4 - 4 * here + j), at], g_blocks.at[j // 2, block(place4), at],
             group_of(to_back), g_recv.at[c], (gate_of(j), t),
         )
 
     def row_copy(c, i):
-        at = pl.ds(c * cols, cols)
+        at = pl.ds(c * bcols, bcols)
         return remote(
             g_rows.at[i, :, at], g_in.at[:, at], group_of(to_rows), b_in.at[c],
             (4 - 4 * here + 2 * i + line, t),
         )
 
     def start_back(c):
-        at = pl.ds(c * cols, cols)
+        at = pl.ds(c * bcols, bcols)
         if chain:
             for j in range(4):
 
@@ -649,7 +653,7 @@
                 def _():
                     for i in now:
                         near_copy(c, i).start()
-                    for m in range(CHUNKS if c == CHUNKS - 1 else 0):
+                    for m in range(returns if c == returns - 1 else 0):
                         for i in range(1, 4):
                             if i not in now:
                                 near_copy(m, i).start()
@@ -665,7 +669,7 @@
 
     def wait_back(c):
         if chain:
-            got = rt.at[pl.ds(0, 3 * cap + rows), pl.ds(c * cols, cols)]
+            got = rt.at[pl.ds(0, 3 * cap + rows), pl.ds(c * bcols, bcols)]
             remote(got, got, group_of(to_back), b_in.at[c], pair).wait_recv()
         else:
 
@@ -678,7 +682,7 @@
     def merge(c):
         if not chain:
             return
-        at = pl.ds(c * cols, cols)
+        at = pl.ds(c * bcols, bcols)
 
         @pl.when(is_gate)
         def _():
@@ -690,9 +694,9 @@
                 g_rows[i, :, at] = rows_in.astype(bf16)
                 row_copy(c, i).start()
 
-    for c in range(CHUNKS):
+    for c in range(returns):
         k = 2 + c
-        at = pl.ds(c * cols, cols)
+        at = pl.ds(c * bcols, bcols)
         pair_copy(k).wait_recv()
         forward(k)
         wait_forwarded(k)
@@ -701,12 +705,10 @@
             total = total + dot(hid[s], df[s, :, at])
         rt[:, at] = total.astype(bf16)
         start_back(c)
-        if c > 0:
-            merge(c - 1)
+        if c >= lag:
+            merge(c - lag)
         if chain and c == 1:
             start_far(0)
-        if chain and c == FAR_AT:
-            far_shared()
         if chain and c == SPREAD_AT:
             spread_away(False)
         if not chain and c == NORMED_AT:
@@ -719,18 +721,21 @@
                 shared(near(d) + 1 - 2 * b)
                 pair_sum(1, lax.rem(a + half - d, half)).start()
             start_far(1)
-    merge(CHUNKS - 1)
+    for c in range(returns - lag, returns):
+        merge(c)
+    if chain:
+        far_shared()
 
     if not chain:
         mix = weighted(chosen, expert, own_routes, own_w)
     pair_sum(1, a).wait_recv()
-    for c in range(CHUNKS):
-        if c == CHUNKS - 1:
+    for c in range(returns):
+        if c == returns - 1:
             pair_sum(0, a).wait_recv()
             for m in range(CHUNKS):
                 at = pl.ds(m * cols, cols)
                 mix_o[:, at] = summed(0, m).astype(bf16)
-        at = pl.ds(c * cols, cols)
+        at = pl.ds(c * bcols, bcols)
         wait_back(c)
         if chain:
             got = rv[pl.ds(pl.multiple_of(here * wide, wide), wide), at]
@@ -738,7 +743,7 @@
             routed = routed + g_in[:, at].astype(f32)
         else:
             routed = dot(mix[0], rv[:, at]) + dot(mix[1], rv[:, at])
-        exp_o[:, at] = (summed(1, c) + routed).astype(bf16)
+        exp_o[:, at] = ((own_shared(at) if chain else summed(1, c)) + routed).astype(bf16)
 
 
     for c in halos:
@@ -802,7 +807,8 @@
     cap = 2 * rows * routes.shape[1] // ep
     cap = -(-cap // 16) * 16
     slots = ep * cap
-    kinds = CHUNKS + 3
+    returns = RETURNS if ep <= 8 else CHUNKS
+    kinds = returns + 3
     vmem = pl.BlockSpec(memory_space=pltpu.VMEM)
     any_spec = pl.BlockSpec(memory_space=pl.ANY)
     dma = pltpu.SemaphoreType.DMA
@@ -832,7 +838,7 @@
         pltpu.VMEM((2, routes.shape[1], rows), f32),
         buf(2, 4 * cap, width), buf(2, rows, width), buf(rows, width),
         buf(2, 2, rows, 4 * cap), buf(2, 2, rows, 4 * cap),
-        dma((2,)), dma((CHUNKS,)), dma((CHUNKS,)),
+        dma((2,)), dma((returns,)), dma((returns,)),
         buf(2, rows, width), buf(2, 4 * cap, width), buf(2, 4 * cap, rows),
         dma((CHUNKS,)), dma((CHUNKS,)),
         buf(half - 1, width, sh_units), buf(half - 1, width, sh_units), buf(half - 1, sh_units, width),

time: 105 us -> 104 us (level)
  the two profiles are of different devices: /device:TPU:17 before, /device:TPU:0 now
where the time goes in v3:
time: 104 us; the launch traced here: 103 us
  Pallas kernels  100 us (96%)
  local copies, waits for them, and re-layouts  1.59 us (2%)
    pallas_call x1, Pallas kernels, per_device(): pl.pallas_call(functools.partial(kernel, (ep, tp, cap)), out_shape=(out,...  100 us

profile of v3, /device:TPU:0, one launch (start us, length us, event | category | flops | bytes accessed | tf_op | source)
XLA Modules:
  0.0 102.5 jit_solution(3581464997548371710)
XLA Ops:
  0.6 100.3 %shard_map.158 = (bf16[128,2048]{1,0:T(8,128)(2,1)S(1)}, bf16[128,2048]{1,0:T(8,128)(2,1)S(1)}) custom-call(bf16[512,512]{1,0:T(8,128)(2,1)} %outer.1, bf16[512,512]{1,0:T(8,128)(2,1)} %inner.1, bf16[512,512]{1,0:T(8,128)(2,1)} %values.1, bf16[3,512]{1,0:T(4,128)(2,1)} %taps.1, bf16[512,2048]{1,0:T(8,128)(2,1)} %out_w.1, bf16[128,2048]{1,0:T(8,128)(2,1)} %tokens.1, ...), custom_call_target="tpu_custom_call" | custom-call | tf_op jit(solution)/shard_map/pallas_call | solution.py:850
  100.9 0.8 copy.19
  101.7 0.8 copy.20

commit v4 on v3

--- a/solution.py
+++ b/solution.py
@@ -647,7 +647,7 @@
                 def _():
                     g_blocks[j // 2, block(place4), at] = rt[block(4 - 4 * here + j), at]
 
-            for gate, now in ((True, (2, 3)), (False, (1,))):
+            for gate, now in ((True, (2,)), (False, (1,))):
 
                 @pl.when(is_gate if gate else jnp.logical_not(is_gate))
                 def _():

time: 104 us -> 104 us (level)
  no operation moved by 1% of the time
where the time goes in v4:
time: 104 us; the launch traced here: 103 us
  Pallas kernels  101 us (97%)
  local copies, waits for them, and re-layouts  1.59 us (2%)
    pallas_call x1, Pallas kernels, per_device(): pl.pallas_call(functools.partial(kernel, (ep, tp, cap)), out_shape=(out,...  101 us

profile of v4, /device:TPU:0, one launch (start us, length us, event | category | flops | bytes accessed | tf_op | source)
XLA Modules:
  0.0 103.3 jit_solution(6697265773020534736)
XLA Ops:
  0.6 101.1 %shard_map.158 = (bf16[128,2048]{1,0:T(8,128)(2,1)S(1)}, bf16[128,2048]{1,0:T(8,128)(2,1)S(1)}) custom-call(bf16[512,512]{1,0:T(8,128)(2,1)} %outer.1, bf16[512,512]{1,0:T(8,128)(2,1)} %inner.1, bf16[512,512]{1,0:T(8,128)(2,1)} %values.1, bf16[3,512]{1,0:T(4,128)(2,1)} %taps.1, bf16[512,2048]{1,0:T(8,128)(2,1)} %out_w.1, bf16[128,2048]{1,0:T(8,128)(2,1)} %tokens.1, ...), custom_call_target="tpu_custom_call" | custom-call | tf_op jit(solution)/shard_map/pallas_call | solution.py:850
  101.8 0.8 copy.19
  102.6 0.8 copy.20
